TPU v7x, 32 devices: a whole 2x2x4 slice. The times are simulated.
32 devices in a mesh: kv: 8 (over z, x), tp: 4 (over y, core).
Axes of the slice: x: 2, y: 2, z: 4, core: 2. Of those that a mesh axis runs over, the one named last changes fastest.
Arguments:
- hidden: bfloat16 [128, 4, 2048], P(None, None, 'kv'), may hold values from -18 to 18
- norm_gain: float32 [2048], replicated, may hold values from 0.1 to 1.9
- w_query: bfloat16 [2048, 1024], P(None, 'tp'), may hold values from -0.125 to 0.125
- w_forget: bfloat16 [2048, 1024], P(None, 'tp'), may hold values from -0.125 to 0.125
- w_input: bfloat16 [2048, 1024], P(None, 'tp'), may hold values from -0.125 to 0.125
- w_outgate: bfloat16 [2048, 1024], P(None, 'tp'), may hold values from -0.125 to 0.125
- w_out: bfloat16 [1024, 2048], replicated, may hold values from -0.1875 to 0.1875
- floor: float32 [1024], P('tp'), may hold values from 0 to 0.95
- head_gain: float32 [128], replicated, may hold values from 0.1 to 1.9
- base_state: float32 [128, 8, 128, 128], P('kv', 'tp'), may hold values from -4 to 4
- prev_forget: bfloat16 [128, 4, 1024], P('kv', None, 'tp'), may hold values from -6 to 6
- prev_input: bfloat16 [128, 4, 1024], P('kv', None, 'tp'), may hold values from -6 to 6
- accepted: int32 [128], P('kv'), may hold values from 0 to 4
Outputs:
- mixed: bfloat16 [128, 4, 2048], P(None, None, 'kv')
- taken_state: float32 [128, 8, 128, 128], P('kv', 'tp')
All inputs are finite; a program needn't handle non-finite values.
Results may differ from a plain program's by a relative error of at most 0.014.
Values may be sent and summed in bfloat16 or wider, within the bound.
A program may use at most 64 MiB of HBM per device.

v0:
```python
import jax
import jax.numpy as jnp
from jax import lax
from jax.sharding import PartitionSpec as P

D = 2048
HEAD_DIM = 128
PROPS = 4


def shards(
    hidden,
    norm_gain,
    w_query,
    w_forget,
    w_input,
    w_outgate,
    w_out,
    floor,
    head_gain,
    base_state,
    prev_forget,
    prev_input,
    accepted,
):
    arrived = lax.all_to_all(hidden, "kv", split_axis=0, concat_axis=2, tiled=True)
    whole_vals = arrived.astype(jnp.float32)
    row_sums = jnp.sum(whole_vals * whole_vals, axis=2)
    normed = (whole_vals * lax.rsqrt(row_sums / D + 1e-06)[..., None] * norm_gain).astype(
        jnp.bfloat16
    )
    query_pre = jnp.dot(normed, w_query, preferred_element_type=jnp.float32).astype(jnp.bfloat16)
    forget_pre = jnp.dot(normed, w_forget, preferred_element_type=jnp.float32).astype(jnp.bfloat16)
    input_pre = jnp.dot(normed, w_input, preferred_element_type=jnp.float32).astype(jnp.bfloat16)
    gate_pre = jnp.dot(normed, w_outgate, preferred_element_type=jnp.float32).astype(jnp.bfloat16)
    seq_local = normed.shape[0]
    head_local = w_query.shape[1] // HEAD_DIM
    shape = (seq_local, PROPS, head_local, HEAD_DIM)
    query = jax.nn.silu(query_pre.astype(jnp.float32)).reshape(shape)
    forget = (floor + (1.0 - floor) * jax.nn.sigmoid(forget_pre.astype(jnp.float32))).reshape(shape)
    value = input_pre.astype(jnp.float32).reshape(shape)
    prev_f = (floor + (1.0 - floor) * jax.nn.sigmoid(prev_forget.astype(jnp.float32))).reshape(
        shape
    )
    prev_v = prev_input.astype(jnp.float32).reshape(shape)
    state = base_state
    for step in range(PROPS):
        live = (step < accepted)[:, None, None, None]
        moved = (
            prev_f[:, step][..., None] * state
            + (1.0 - prev_f[:, step])[..., None] * prev_v[:, step][:, :, None, :]
        )
        state = jnp.where(live, moved, state)
    taken_state = state
    outputs = []
    for step in range(PROPS):
        state = (
            forget[:, step][..., None] * state
            + (1.0 - forget[:, step])[..., None] * value[:, step][:, :, None, :]
        )
        outputs.append(
            jnp.einsum("bhk,bhkv->bhv", query[:, step], state, precision=lax.Precision.HIGHEST)
        )
    result = jnp.stack(outputs, axis=1)
    scaled = (
        result * lax.rsqrt(jnp.mean(result * result, axis=-1, keepdims=True) + 1e-05) * head_gain
    )
    gated = scaled * jax.nn.silu(gate_pre.astype(jnp.float32)).reshape(shape)
    mixed_heads = gated.reshape(seq_local, PROPS, head_local * HEAD_DIM).astype(jnp.bfloat16)
    own_rows = mixed_heads.shape[2]
    w_rows = lax.dynamic_slice_in_dim(w_out, lax.axis_index("tp") * own_rows, own_rows, 0)
    partial_value = jnp.dot(mixed_heads, w_rows, preferred_element_type=jnp.float32)
    finished = lax.psum(partial_value, "tp").astype(jnp.bfloat16)
    mixed = lax.all_to_all(finished, "kv", split_axis=2, concat_axis=0, tiled=True)
    return (mixed, taken_state)


def solution(mesh):
    placed = (
        P(None, None, "kv"),
        P(),
        P(None, "tp"),
        P(None, "tp"),
        P(None, "tp"),
        P(None, "tp"),
        P(),
        P("tp"),
        P(),
        P("kv", "tp", None, None),
        P("kv", None, "tp"),
        P("kv", None, "tp"),
        P("kv"),
    )
    return jax.shard_map(
        shards,
        mesh=mesh,
        in_specs=placed,
        out_specs=(P(None, None, "kv"), P("kv", "tp", None, None)),
        check_vma=False,
    )
```

profile of v0, /device:TPU:0, one launch (start us, length us, event | category | flops | bytes accessed | tf_op | source)
XLA Modules:
  0.0 96.0 jit_solution(18002514994027775703)
XLA Ops:
  0.6 0.0 copy-start
  0.6 7.4 %all-to-all-start = ((bf16[128,4,256]{2,1,0:T(4,128)(2,1)}), bf16[128,4,256]{2,1,0:T(4,128)(2,1)S(1)}, u32[]{:S(2)}, u32[]{:S(2)}) async-start(bf16[128,4,256]{2,1,0:T(4,128)(2,1)} %param.13), calls=%async_computation | async-start | bytes 524288 | tf_op jit(solution)/shard_map/all_to_all | solution.py:26
  8.1 0.7 broadcast_subtract_fusion.8
  8.8 0.6 copy-done.3
  9.3 0.8 multiply_add_fusion.9
  10.2 1.2 %broadcast_bitcast_fusion = f32[256]{0:T(256)} fusion(f32[128]{0:T(128)} %param.21), kind=kLoop, calls=%fused_computation.82 | loop fusion | bytes 1536 | tf_op jit(solution)/shard_map/mul | solution.py:66
  11.5 1.3 %broadcast_compare_fusion.3 = (pred[16]{0:T(512)(128)(4,1)}, pred[16]{0:T(512)(128)(4,1)}, pred[16]{0:T(512)(128)(4,1)}, pred[16]{0:T(512)(128)(4,1)}) fusion(s32[16]{0:T(128)} %param.25), kind=kLoop, calls=%fused_computation.88 | loop fusion | flops 64 | bytes 128 | tf_op jit(solution)/shard_map/gt | solution.py:48
  12.7 0.8 reshape.130
  13.5 0.6 slice_bitcast_fusion.10
  14.1 7.1 %add_select_fusion = f32[16,2,128,128]{3,2,1,0:T(8,128)S(1)} fusion(f32[16,2,128,128]{3,2,1,0:T(8,128)} %param.22, f32[16,2,128]{2,1,0:T(2,128)} %get-tuple-element.29, f32[16,2,128]{2,1,0:T(2,128)S(1)} %get-tuple-element.25, f32[16,2,128]{2,1,0:T(2,128)} %get-tuple-element.27, f32[16,2,128]{2,1,0:T(2,128)S(1)} %get-tuple-element.24, ...), kind=kLoop, calls=%fused_computation.7 | loop fusion | flops 8388608 | bytes 4390976 | tf_op jit(solution)/shard_map/jit(_where)/select_n | solution.py:53
  21.3 0.0 copy-start.1
  21.3 0.0 copy-start.5
  21.3 0.0 copy-start.2
  21.3 0.0 copy-start.4
  21.3 0.0 all-to-all-done
  21.3 0.2 multiply_reduce_fusion
  21.6 0.1 copy.55
  21.7 0.1 convert_element_type.70
  21.7 1.1 %copy.38 = f32[16,4,8,256]{3,2,0,1:T(8,128)} copy(f32[16,4,8,256]{3,1,0,2:T(4,128)S(1)} %bitcast.141) | data formatting | bytes 1048576 | tf_op jit(solution)/shard_map/convert_element_type | solution.py:27
  22.8 1.9 %reshape.128 = f32[16,4,2048]{2,0,1:T(8,128)} reshape(f32[16,4,8,256]{3,2,0,1:T(8,128)} %copy.38) | data formatting | bytes 1048576 | tf_op jit(solution)/shard_map/convert_element_type | solution.py:27
  24.8 0.0 copy-done.5
  24.8 1.2 %multiply_convert_fusion = bf16[16,4,2048]{2,0,1:T(8,128)(2,1)S(1)} fusion(f32[16,4,2048]{2,0,1:T(8,128)} %reshape.128, f32[2048]{0:T(1024)S(1)} %copy-done.5, f32[16,4]{0,1:T(4,128)S(1)} %add_rsqrt_fusion.1), kind=kLoop, calls=%fused_computation.43 | loop fusion | flops 393216 | bytes 794880 | tf_op jit(solution)/shard_map/convert_element_type | solution.py:29
  25.9 0.0 copy-done.2
  25.9 0.0 copy-done.4
  25.9 1.5 %fusion.14 = f32[16,4,256]{2,0,1:T(8,128)S(1)} fusion(bf16[16,4,2048]{2,0,1:T(8,128)(2,1)S(1)} %multiply_convert_fusion, bf16[2048,256]{1,0:T(8,128)(2,1)} %param.16, f32[256]{0:T(256)S(1)} %copy-done.4, f32[256]{0:T(256)S(1)} %copy-done.2), kind=kOutput, calls=%fused_computation.21 | convolution fusion | flops 67223552 | bytes 1378304 | tf_op jit(solution)/shard_map/dot_general | solution.py:33
  27.5 1.5 %fusion.7 = f32[16,4,256]{2,0,1:T(8,128)S(1)} fusion(bf16[16,4,2048]{2,0,1:T(8,128)(2,1)S(1)} %multiply_convert_fusion, bf16[2048,256]{1,0:T(8,128)(2,1)} %param.17), kind=kOutput, calls=%fused_computation.13 | convolution fusion | flops 67141632 | bytes 1376256 | tf_op jit(solution)/shard_map/dot_general | solution.py:34
  29.1 0.7 reshape.132
  29.7 2.2 %divide_multiply_fusion = f32[16,4,256]{2,0,1:T(8,128)} fusion(bf16[16,4,2048]{2,0,1:T(8,128)(2,1)S(1)} %multiply_convert_fusion, bf16[2048,256]{1,0:T(8,128)(2,1)} %param.15), kind=kOutput, calls=%fused_computation.53 | convolution fusion | flops 67207168 | bytes 1376256 | tf_op jit(solution)/shard_map/dot_general | solution.py:32
  31.9 0.9 reshape.121
  32.8 0.8 slice_bitcast_fusion.6
  33.6 2.8 %fusion.4 = f32[16,2,1,128]{3,2,1,0:T(1,128)S(1)} fusion(f32[16,2,128,1]{2,3,1,0:T(1,128)S(1)} %bitcast.146, f32[16,2,128,128]{3,2,1,0:T(8,128)S(1)} %add_select_fusion, f32[16,2,128]{2,1,0:T(2,128)S(1)} %get-tuple-element.14, f32[16,2,128]{2,1,0:T(2,128)S(1)} %get-tuple-element.10, f32[16,2,128]{2,1,0:T(2,128)S(1)} %get-tuple-element.37), kind=kOutput, calls=%fused_computation.8 | convolution fusion | flops 7864320 | bytes 2179072 | tf_op jit(solution)/shard_map/bhk,bhkv->bhv/dot_general | solution.py:62
  36.4 4.3 %fusion.35 = f32[16,2,1,128]{3,2,1,0:T(1,128)S(1)} fusion(f32[16,2,128,1]{2,3,1,0:T(1,128)S(1)} %bitcast.155, f32[16,2,128,128]{3,2,1,0:T(8,128)S(1)} %add_select_fusion, f32[16,2,128]{2,1,0:T(2,128)S(1)} %get-tuple-element.17, f32[16,2,128]{2,1,0:T(2,128)S(1)} %get-tuple-element.13, f32[16,2,128]{2,1,0:T(2,128)S(1)} %get-tuple-element.34, ...), kind=kOutput, calls=%fused_computation.45 | convolution fusion | flops 9437184 | bytes 2228224 | tf_op jit(solution)/shard_map/bhk,bhkv->bhv/dot_general | solution.py:62
  40.7 6.1 %fusion.5 = f32[16,2,1,128]{3,2,1,0:T(1,128)S(1)} fusion(f32[16,2,128,1]{2,3,1,0:T(1,128)S(1)} %bitcast.154, f32[16,2,128]{2,1,0:T(2,128)S(1)} %get-tuple-element.16, f32[16,2,128]{2,1,0:T(2,128)S(1)} %get-tuple-element.12, f32[16,2,128]{2,1,0:T(2,128)S(1)} %get-tuple-element.35, f32[16,2,128,128]{3,2,1,0:T(8,128)S(1)} %add_select_fusion, ...), kind=kOutput, calls=%fused_computation.9 | convolution fusion | flops 11010048 | bytes 2277376 | tf_op jit(solution)/shard_map/bhk,bhkv->bhv/dot_general | solution.py:62
  46.8 0.0 copy-done.1
  46.8 0.0 copy-start.6
  46.8 7.2 %fusion = f32[16,2,1,128]{3,2,1,0:T(1,128)S(1)} fusion(f32[16,2,128,1]{2,3,1,0:T(1,128)S(1)} %bitcast.153, f32[16,2,128]{2,1,0:T(2,128)S(1)} %get-tuple-element.15, f32[16,2,128]{2,1,0:T(2,128)S(1)} %get-tuple-element.11, f32[16,2,128]{2,1,0:T(2,128)S(1)} %get-tuple-element.36, f32[16,2,128]{2,1,0:T(2,128)S(1)} %get-tuple-element.16, ...), kind=kOutput, calls=%fused_computation | convolution fusion | flops 12582912 | bytes 2326528 | tf_op jit(solution)/shard_map/bhk,bhkv->bhv/dot_general | solution.py:62
  54.1 0.1 fusion.39
  54.2 0.1 mul.343
  54.4 0.1 mul.344
  54.4 0.0 copy-done
  54.4 0.0 copy-done.6
  54.4 2.0 %fusion.16 = f32[16,4,2048]{2,0,1:T(8,128)S(1)} fusion(bf16[1024,2048]{1,0:T(8,128)(2,1)} %param.19, s32[]{:T(128)S(6)} %select_n.20, f32[16,4,256]{2,0,1:T(8,128)S(1)} %mul.344, f32[16,1,256]{2,0,1:T(8,128)S(1)} %stack.28, f32[16,1,256]{2,0,1:T(8,128)S(1)} %stack.27, f32[16,1,256]{2,0,1:T(8,128)S(1)} %stack.26, f32[16,1,256]{2,0,1:T(8,128)S(1)} %stack.25, ...), kind=kOutput, calls=%fused_computation.24 | convolution fusion | flops 134430720 | bytes 3015684 | tf_op jit(solution)/shard_map/dot_general | solution.py:72
  56.5 16.6 %all-reduce.1 = bf16[16,4,2048]{2,0,1:T(8,128)(2,1)S(1)} all-reduce(f32[16,4,2048]{2,0,1:T(8,128)S(1)} %fusion.16), channel_id=1, replica_groups=mesh['kv'=8,'tp'=4] {'tp'}, use_global_device_ids=true, to_apply=%region_3.4 | all-reduce | flops 131072 | bytes 786432 | tf_op jit(solution)/shard_map/psum | solution.py:73
  73.1 1.4 %copy.45 = bf16[16,4,2048]{0,1,2:T(4,128)(2,1)S(1)} copy(bf16[16,4,2048]{2,0,1:T(8,128)(2,1)S(1)} %all-reduce.1) | data formatting | bytes 524288 | tf_op jit(solution)/shard_map/convert_element_type | solution.py:73
  74.5 2.2 %reshape.148 = bf16[8,2,8192]{2,1,0:T(2,128)(2,1)S(1)} reshape(bf16[2048,4,16]{2,1,0:T(4,128)(2,1)S(1)} %bitcast.139) | data formatting | bytes 524288
  76.7 14.9 %all_to_all.27 = bf16[8,2,8192]{2,1,0:T(2,128)(2,1)} all-to-all(bf16[8,2,8192]{2,1,0:T(2,128)(2,1)S(1)} %reshape.148), channel_id=1, replica_groups=mesh['kv'=8,'tp'=4] {'kv'}, dimensions={0} | all-to-all | bytes 524288 | tf_op jit(solution)/shard_map/all_to_all | solution.py:74
  91.5 2.4 %reshape.149 = bf16[2048,4,16]{2,1,0:T(4,128)(2,1)S(1)} reshape(bf16[8,2,8192]{2,1,0:T(2,128)(2,1)} %all_to_all.27) | data formatting | bytes 524288
  94.0 2.0 %copy.46 = bf16[8,16,4,256]{3,2,1,0:T(4,128)(2,1)} copy(bf16[8,16,4,256]{1,2,3,0:T(4,128)(2,1)S(1)} %bitcast.140) | data formatting | bytes 524288 | tf_op jit(solution)/shard_map/all_to_all | solution.py:74
  (14 shorter events, 0.3 us)
Async XLA Ops:
  0.6 53.8 %copy-start = (bf16[2048,256]{1,0:T(8,128)(2,1)S(1)}, bf16[2048,256]{1,0:T(8,128)(2,1)}, u32[]{:S(2)}) copy-start(bf16[2048,256]{1,0:T(8,128)(2,1)} %param.18) | copy-start | bytes 3145732
  0.6 20.7 %all-to-all-start = ((bf16[128,4,256]{2,1,0:T(4,128)(2,1)}), bf16[128,4,256]{2,1,0:T(4,128)(2,1)S(1)}, u32[]{:S(2)}, u32[]{:S(2)}) async-start(bf16[128,4,256]{2,1,0:T(4,128)(2,1)} %param.13), calls=%async_computation | async-start | bytes 524288 | tf_op jit(solution)/shard_map/all_to_all | solution.py:26
  8.8 0.6 copy-start.3
  21.3 25.5 %copy-start.1 = (f32[16,2,128,128]{3,2,1,0:T(8,128)}, f32[16,2,128,128]{3,2,1,0:T(8,128)S(1)}, u32[]{:S(2)}) copy-start(f32[16,2,128,128]{3,2,1,0:T(8,128)S(1)} %add_select_fusion) | copy-start | bytes 6291460
  21.3 3.5 %copy-start.5 = (f32[2048]{0:T(1024)S(1)}, f32[2048]{0:T(1024)}, u32[]{:S(2)}) copy-start(f32[2048]{0:T(1024)} %param.14) | copy-start | bytes 24580
  21.3 4.6 %copy-start.2 = (f32[256]{0:T(256)S(1)}, f32[256]{0:T(256)}, u32[]{:S(2)}) copy-start(f32[256]{0:T(256)} %param.20) | copy-start | bytes 3076
  21.3 4.6 %copy-start.4 = (f32[256]{0:T(256)S(1)}, f32[256]{0:T(256)}, u32[]{:S(2)}) copy-start(f32[256]{0:T(256)} %copy-done.3) | copy-start | bytes 3076
  46.8 7.7 %copy-start.6 = (f32[256]{0:T(256)S(1)}, f32[256]{0:T(256)}, u32[]{:S(2)}) copy-start(f32[256]{0:T(256)} %broadcast_bitcast_fusion) | copy-start | bytes 3076
where the time goes:
time: 96.9 us; the launch traced here: 96 us
  blocking collectives  31.5 us (33%)
  matrix products  27.6 us (28%)
  local copies, waits for them, and re-layouts  17 us (18%)
  other arithmetic  11.5 us (12%)
  starting transfers between devices  7.42 us (8%)
    dot_general x4, matrix products, shards(): jnp.einsum('bhk,bhkv->bhv', query[:, step], state, precision=lax.Precisio...  20.3 us
    psum x1, blocking collectives, shards(): finished = lax.psum(partial_value, 'tp').astype(jnp.bfloat16)  16.6 us
    all_to_all x1, blocking collectives, shards(): lax.all_to_all(finished, 'kv', split_axis=2, concat_axis=0, tiled=True)  14.9 us
    all_to_all x1, starting transfers between devices, shards(): lax.all_to_all(hidden, 'kv', split_axis=0, concat_axis=2, tiled=True)  7.42 us
    select_n x1, other arithmetic, shards(): state = jnp.where(live, moved, state)  7.13 us
    unnamed x17, local copies, waits for them, and re-layouts  5.27 us
    convert_element_type x2, local copies, waits for them, and re-layouts, shards(): whole_vals = arrived.astype(jnp.float32)  3.03 us
    dot_general x1, matrix products, shards(): jnp.dot(normed, w_query, preferred_element_type=jnp.float32)  2.17 us
  transfers between devices with their start and end apart: 1, of which 0 were waited for; matrix products, arithmetic and copies ran while one was open for 13% of the time, Pallas kernels for 0%

commit v1 on v0

--- a/solution.py
+++ b/solution.py
@@ -1,6 +1,10 @@
+import functools
+
 import jax
 import jax.numpy as jnp
 from jax import lax
+from jax.experimental import pallas as pl
+from jax.experimental.pallas import tpu as pltpu
 from jax.sharding import PartitionSpec as P
 
 D = 2048
@@ -75,6 +79,419 @@
     return (mixed, taken_state)
 
 
+def fused_kernel(
+    n_kv,
+    n_tp,
+    accepted,
+    hidden,
+    gain,
+    w_query,
+    w_forget,
+    w_input,
+    w_outgate,
+    w_out,
+    floor,
+    head_gain,
+    base_state,
+    prev_forget,
+    prev_input,
+    out,
+    taken,
+    hid,
+    arrived,
+    gain_v,
+    w_all,
+    w_o,
+    floor_v,
+    head_gain_v,
+    state,
+    state16,
+    prev_f_v,
+    prev_i_v,
+    acc,
+    heads_all,
+    blocks,
+    landed,
+    local_sem,
+    wo_sem,
+    taken_sem,
+    in_send,
+    in_recv,
+    fwd_send,
+    fwd_recv,
+    tp_send,
+    tp_recv,
+    out_send,
+    out_recv,
+    ofwd_send,
+    ofwd_recv,
+):
+    f32, bf16 = jnp.float32, jnp.bfloat16
+    seqs, props = hid.shape[0] // n_kv, hid.shape[1]
+    cols = hid.shape[2]
+    rows = seqs * props
+    half_seq = seqs // 2
+    width = w_query.shape[1]
+    head_local = width // HEAD_DIM
+    half_cols = cols // 2
+    depth = n_kv * cols
+    kv, tp = lax.axis_index("kv"), lax.axis_index("tp")
+    core = lax.rem(tp, 2)
+    peer = tp + 1 - 2 * core
+
+    locals_ = [
+        pltpu.make_async_copy(hidden, hid, local_sem.at[0]),
+        pltpu.make_async_copy(prev_forget, prev_f_v, local_sem.at[1]),
+        pltpu.make_async_copy(prev_input, prev_i_v, local_sem.at[2]),
+        pltpu.make_async_copy(floor, floor_v, local_sem.at[3]),
+        pltpu.make_async_copy(base_state, state, local_sem.at[4]),
+        pltpu.make_async_copy(gain, gain_v, local_sem.at[5]),
+        pltpu.make_async_copy(head_gain, head_gain_v, local_sem.at[6]),
+    ]
+    for place, weight in enumerate((w_query, w_forget, w_input, w_outgate)):
+        locals_.append(
+            pltpu.make_async_copy(
+                weight, w_all.at[:, pl.ds(place * width, width)], local_sem.at[7 + place]
+            )
+        )
+    w_o_copies = [
+        pltpu.make_async_copy(
+            w_out.at[:, pl.ds(pl.multiple_of(k * cols + core * half_cols, half_cols), half_cols)],
+            w_o.at[:, pl.ds(k * half_cols, half_cols)],
+            wo_sem.at[k],
+        )
+        for k in range(n_kv)
+    ]
+    barrier = pltpu.get_barrier_semaphore()
+    for step in range(1, n_kv):
+        pl.semaphore_signal(
+            barrier,
+            inc=1,
+            device_id={"kv": lax.rem(kv + step, n_kv)},
+            device_id_type=pl.DeviceIdType.MESH,
+        )
+    for step in range(1, n_tp):
+        pl.semaphore_signal(
+            barrier,
+            inc=1,
+            device_id={"tp": lax.rem(tp + step, n_tp)},
+            device_id_type=pl.DeviceIdType.MESH,
+        )
+    for copy in locals_:
+        copy.start()
+    for copy in w_o_copies:
+        copy.start()
+    locals_[0].wait()
+    pl.semaphore_wait(barrier, n_kv + n_tp - 2)
+
+    def remote(source, target, send, recv, device):
+        return pltpu.make_async_remote_copy(
+            src_ref=source,
+            dst_ref=target,
+            send_sem=send,
+            recv_sem=recv,
+            device_id=device,
+            device_id_type=pl.DeviceIdType.MESH,
+        )
+
+    order = sorted(range(1, n_kv), key=lambda step: -min(step, n_kv - step))
+    mine = pl.ds(core * half_seq, half_seq)
+    in_copies = {}
+    for step in order:
+        to = lax.rem(kv + step, n_kv)
+        in_copies[step] = remote(
+            hid.at[pl.ds(to * seqs + core * half_seq, half_seq)],
+            arrived.at[kv, mine],
+            in_send.at[step],
+            in_recv.at[step],
+            {"kv": to},
+        )
+        in_copies[step].start()
+
+    for copy in locals_[1:5]:
+        copy.wait()
+    low = floor_v[...]
+    row = lax.broadcasted_iota(jnp.int32, (rows, width), 0)
+    at = lax.rem(row, props)
+    seq_of = lax.div(row, props)
+    taken_count = jnp.zeros((rows, width), jnp.int32)
+    for s in range(seqs):
+        taken_count = jnp.where(seq_of == s, accepted[s], taken_count)
+    live = at < taken_count
+    prev_f = low + (1.0 - low) * jax.nn.sigmoid(
+        prev_f_v[...].astype(f32).reshape(rows, width)
+    )
+    prev_v = prev_i_v[...].astype(f32).reshape(rows, width)
+    decay = jnp.where(live, prev_f, 1.0)
+    enter = jnp.where(live, 1.0 - prev_f, 0.0)
+    later = jnp.ones((rows, width), f32)
+    for lag in range(1, props):
+        later = later * jnp.where(
+            at < props - lag, pltpu.roll(decay, rows - lag, axis=0), 1.0
+        )
+    enter = enter * later
+    whole = jnp.where(at == 0, decay * later, 0.0)
+
+    def split(x):
+        high = x.astype(bf16).astype(f32)
+        return high, x - high
+
+    coeffs = jnp.concatenate(split(enter) + split(whole), axis=0)
+    seq_row = lax.div(
+        lax.rem(lax.broadcasted_iota(jnp.int32, (2 * rows, HEAD_DIM), 0), rows), props
+    )
+    nothing = jnp.zeros((2 * rows, HEAD_DIM), f32)
+    left, values = [], []
+    for h in range(head_local):
+        part = slice(h * HEAD_DIM, (h + 1) * HEAD_DIM)
+        left.append(coeffs[:, part].T.astype(bf16))
+        values.append(jnp.concatenate([prev_v[:, part]] * 2, axis=0))
+
+    def take(s, carry):
+        own = seq_row == s
+        for h in range(head_local):
+            right = jnp.concatenate(
+                [
+                    jnp.concatenate([jnp.where(own, values[h], 0.0), nothing], axis=1),
+                    jnp.concatenate([nothing, jnp.where(own, 1.0, 0.0)], axis=1),
+                ],
+                axis=0,
+            ).astype(bf16)
+            both = jnp.dot(left[h], right, preferred_element_type=f32)
+            fresh = both[:, HEAD_DIM:] * state[s, h] + both[:, :HEAD_DIM]
+            state[s, h] = fresh
+            state16[h, :, pl.ds(pl.multiple_of(s * HEAD_DIM, HEAD_DIM), HEAD_DIM)] = fresh.astype(
+                bf16
+            )
+        return carry
+
+    lax.fori_loop(0, seqs, take, 0)
+    taken_copy = pltpu.make_async_copy(state, taken, taken_sem)
+    taken_copy.start()
+    for copy in locals_[5:]:
+        copy.wait()
+
+    def project(source, block, first):
+        x = block.astype(f32).reshape(rows, cols)
+        lanes = pl.ds(pl.multiple_of(source * cols, cols), cols)
+        scaled = (x * gain_v[:, lanes]).astype(bf16)
+        term = jnp.dot(scaled, w_all[lanes, :], preferred_element_type=f32)
+        if first:
+            acc[...] = term
+        else:
+            acc[...] += term
+        return jnp.sum(x * x, axis=1, keepdims=True)
+
+    squares = project(kv, hid[pl.ds(kv * seqs, seqs)], True)
+    fwd_copies = {}
+    for place, step in enumerate(order):
+        source = lax.rem(kv + n_kv - step, n_kv)
+        in_copies[step].wait_recv()
+        fwd_copies[step] = remote(
+            arrived.at[source, mine],
+            arrived.at[source, mine],
+            fwd_send.at[step],
+            fwd_recv.at[step],
+            {"tp": peer},
+        )
+        fwd_copies[step].start()
+        if place:
+            step = order[place - 1]
+            source = lax.rem(kv + n_kv - step, n_kv)
+            fwd_copies[step].wait_recv()
+            squares += project(source, arrived[source], False)
+    step = order[-1]
+    source = lax.rem(kv + n_kv - step, n_kv)
+    fwd_copies[step].wait_recv()
+    squares += project(source, arrived[source], False)
+
+    scale = lax.rsqrt(squares / depth + 1e-06)
+    pre = [
+        (acc[:, place * width : (place + 1) * width] * scale).astype(bf16).astype(f32)
+        for place in range(4)
+    ]
+    query = jax.nn.silu(pre[0])
+    forget = low + (1.0 - low) * jax.nn.sigmoid(pre[1])
+    key = 1.0 - forget
+    value = pre[2]
+    gate = jax.nn.silu(pre[3])
+    shifted = [forget] + [pltpu.roll(forget, lag, axis=0) for lag in range(1, props)]
+    reach = forget
+    for lag in range(1, props):
+        reach = reach * jnp.where(at >= lag, shifted[lag], 1.0)
+    from_state = (query * reach).astype(bf16)
+    near = []
+    walk = query
+    for lag in range(props):
+        if lag:
+            walk = walk * shifted[lag - 1]
+            near.append(
+                (
+                    jnp.where(at >= lag, walk * pltpu.roll(key, lag, axis=0), 0.0),
+                    pltpu.roll(value, lag, axis=0),
+                )
+            )
+        else:
+            near.append((walk * key, value))
+    seq_head = lax.div(lax.broadcasted_iota(jnp.int32, (rows, HEAD_DIM), 0), props)
+    for h in range(head_local):
+        part = slice(h * HEAD_DIM, (h + 1) * HEAD_DIM)
+        every = jnp.dot(from_state[:, part], state16[h], preferred_element_type=f32)
+        o = jnp.zeros((rows, HEAD_DIM), f32)
+        for s in range(seqs):
+            o = jnp.where(seq_head == s, every[:, s * HEAD_DIM : (s + 1) * HEAD_DIM], o)
+        for weight, fresh in near:
+            o += jnp.sum(weight[:, part], axis=1, keepdims=True) * fresh[:, part]
+        size = lax.rsqrt(jnp.mean(o * o, axis=1, keepdims=True) + 1e-05)
+        heads_all[tp, :, part] = (o * size * head_gain_v[...] * gate[:, part]).astype(bf16)
+
+    tp_copies = {}
+    for step in sorted(range(1, n_tp), key=lambda step: -step % 2):
+        to = lax.rem(tp + step, n_tp)
+        tp_copies[step] = remote(
+            heads_all.at[tp], heads_all.at[tp], tp_send.at[step], tp_recv.at[step], {"tp": to}
+        )
+        tp_copies[step].start()
+    for copy in w_o_copies:
+        copy.wait()
+
+    def mix(owner):
+        lines = pl.ds(pl.multiple_of(owner * width, width), width)
+        return jnp.dot(heads_all[owner], w_o[lines, :], preferred_element_type=f32)
+
+    acc_out = mix(tp)
+    for step, copy in tp_copies.items():
+        copy.wait_recv()
+        acc_out += mix(lax.rem(tp + n_tp - step, n_tp))
+    for k in range(n_kv):
+        blocks[k] = acc_out[:, k * half_cols : (k + 1) * half_cols].astype(bf16)
+
+    out_copies = {}
+    for step in order:
+        to = lax.rem(kv + step, n_kv)
+        out_copies[step] = remote(
+            blocks.at[to], landed.at[kv, core], out_send.at[step], out_recv.at[step], {"kv": to}
+        )
+        out_copies[step].start()
+    ofwd = {
+        0: remote(
+            blocks.at[kv], landed.at[kv, core], ofwd_send.at[0], ofwd_recv.at[0], {"tp": peer}
+        )
+    }
+    ofwd[0].start()
+    landed[kv, core] = blocks[kv]
+    for step in order:
+        source = lax.rem(kv + n_kv - step, n_kv)
+        out_copies[step].wait_recv()
+        ofwd[step] = remote(
+            landed.at[source, core],
+            landed.at[source, core],
+            ofwd_send.at[step],
+            ofwd_recv.at[step],
+            {"tp": peer},
+        )
+        ofwd[step].start()
+    for copy in ofwd.values():
+        copy.wait_recv()
+    for k in range(n_kv):
+        out[k * rows : (k + 1) * rows, :] = jnp.concatenate([landed[k, 0], landed[k, 1]], axis=1)
+    for group in (in_copies, fwd_copies, tp_copies, out_copies, ofwd):
+        for copy in group.values():
+            copy.wait_send()
+    taken_copy.wait()
+
+
+def fused(
+    n_kv,
+    n_tp,
+    hidden,
+    norm_gain,
+    w_query,
+    w_forget,
+    w_input,
+    w_outgate,
+    w_out,
+    floor,
+    head_gain,
+    base_state,
+    prev_forget,
+    prev_input,
+    accepted,
+):
+    f32, bf16 = jnp.float32, jnp.bfloat16
+    all_seqs, props, cols = hidden.shape
+    seqs = all_seqs // n_kv
+    rows = seqs * props
+    width = w_query.shape[1]
+    depth = n_kv * cols
+    head_local = width // HEAD_DIM
+    anywhere = pl.BlockSpec(memory_space=pl.ANY)
+    dma = pltpu.SemaphoreType.DMA
+    out, taken = pl.pallas_call(
+        functools.partial(fused_kernel, n_kv, n_tp),
+        out_shape=(
+            jax.ShapeDtypeStruct((all_seqs * props, cols), bf16),
+            jax.ShapeDtypeStruct(base_state.shape, f32),
+        ),
+        in_specs=[pl.BlockSpec(memory_space=pltpu.SMEM)] + [anywhere] * 12,
+        out_specs=(pl.BlockSpec(memory_space=pltpu.VMEM), anywhere),
+        scratch_shapes=[
+            pltpu.VMEM(hidden.shape, bf16),
+            pltpu.VMEM((n_kv, seqs, props, cols), bf16),
+            pltpu.VMEM((1, depth), f32),
+            pltpu.VMEM((depth, 4 * width), bf16),
+            pltpu.VMEM((n_tp * width, depth // 2), bf16),
+            pltpu.VMEM((1, width), f32),
+            pltpu.VMEM((1, HEAD_DIM), f32),
+            pltpu.VMEM(base_state.shape, f32),
+            pltpu.VMEM((head_local, HEAD_DIM, seqs * HEAD_DIM), bf16),
+            pltpu.VMEM(prev_forget.shape, bf16),
+            pltpu.VMEM(prev_input.shape, bf16),
+            pltpu.VMEM((rows, 4 * width), f32),
+            pltpu.VMEM((n_tp, rows, width), bf16),
+            pltpu.VMEM((n_kv, rows, cols // 2), bf16),
+            pltpu.VMEM((n_kv, 2, rows, cols // 2), bf16),
+            dma((11,)),
+            dma((n_kv,)),
+            dma,
+            dma((n_kv,)),
+            dma((n_kv,)),
+            dma((n_kv,)),
+            dma((n_kv,)),
+            dma((n_tp,)),
+            dma((n_tp,)),
+            dma((n_kv,)),
+            dma((n_kv,)),
+            dma((n_kv,)),
+            dma((n_kv,)),
+        ],
+        compiler_params=pltpu.CompilerParams(
+            collective_id=0, has_side_effects=True, vmem_limit_bytes=56 * 1024 * 1024
+        ),
+    )(
+        accepted,
+        hidden,
+        norm_gain.reshape(1, depth),
+        w_query,
+        w_forget,
+        w_input,
+        w_outgate,
+        w_out,
+        floor.reshape(1, width),
+        head_gain.reshape(1, HEAD_DIM),
+        base_state,
+        prev_forget,
+        prev_input,
+    )
+    return out.reshape(hidden.shape), taken
+
+
+def by_shape(n_kv, n_tp, hidden, *rest):
+    if hidden.shape[2] % 256 == 0 and n_tp % 2 == 0:
+        return fused(n_kv, n_tp, hidden, *rest)
+    return shards(hidden, *rest)
+
+
 def solution(mesh):
     placed = (
         P(None, None, "kv"),
@@ -92,7 +509,7 @@
         P("kv"),
     )
     return jax.shard_map(
-        shards,
+        functools.partial(by_shape, mesh.shape["kv"], mesh.shape["tp"]),
         mesh=mesh,
         in_specs=placed,
         out_specs=(P(None, None, "kv"), P("kv", "tp", None, None)),

time: 96.9 us -> 32.1 us (0.33)
  blocking collectives: 31.5 us -> 0 us
  matrix products: 27.6 us -> 0 us
  Pallas kernels: 0 us -> 26.5 us
  local copies, waits for them, and re-layouts: 17 us -> 4.85 us
  other arithmetic: 11.5 us -> 0 us
  starting transfers between devices: 7.42 us -> 0 us
    dot_general x8 -> x0, matrix products: 27.6 us -> none  [the longest x4 20.3 us: shards(): jnp.einsum('bhk,bhkv->bhv', query[:, step], state, precision=lax.Precisio...]
    pallas_call x0 -> x1, Pallas kernels: none -> 26.5 us  [fused(): pl.pallas_call(functools.partial(fused_kernel, n_kv, n_tp), out_shape=(ja...]
    psum x1 -> x0, blocking collectives: 16.6 us -> none  [shards(): finished = lax.psum(partial_value, 'tp').astype(jnp.bfloat16)]
    all_to_all x1 -> x0, blocking collectives: 14.9 us -> none  [shards(): lax.all_to_all(finished, 'kv', split_axis=2, concat_axis=0, tiled=True)]
    all_to_all x1 -> x0, starting transfers between devices: 7.42 us -> none  [shards(): lax.all_to_all(hidden, 'kv', split_axis=0, concat_axis=2, tiled=True)]
    select_n x1 -> x0, other arithmetic: 7.13 us -> none  [shards(): state = jnp.where(live, moved, state)]
    convert_element_type x3 -> x0, local copies, waits for them, and re-layouts: 4.38 us -> none  [the longest x2 3.03 us: shards(): whole_vals = arrived.astype(jnp.float32)]
    mul x6 -> x0, local copies, waits for them, and re-layouts: 2.84 us -> none  [the longest x3 1.42 us: shards(): result * lax.rsqrt(jnp.mean(result * result, axis=-1, keepdims=True) + 1e...]
  transfers between devices with their start and end apart: 1 -> 0, of which waited for: 0 -> 0; matrix products, arithmetic and copies ran while one was open for 13% -> 0% of each run, Pallas kernels for 0% -> 0%
where the time goes in v1:
time: 32.1 us; the launch traced here: 32 us
  Pallas kernels  26.5 us (83%)
  local copies, waits for them, and re-layouts  4.85 us (15%)
  between operations  0.64 us (2%)
    pallas_call x1, Pallas kernels, fused(): pl.pallas_call(functools.partial(fused_kernel, n_kv, n_tp), out_shape=(ja...  26.5 us
    unnamed x1, local copies, waits for them, and re-layouts  3.13 us
    reshape x1, local copies, waits for them, and re-layouts, fused(): return (out.reshape(hidden.shape), taken)  1.72 us

profile of v1, /device:TPU:0, one launch (start us, length us, event | category | flops | bytes accessed | tf_op | source)
XLA Modules:
  0.0 32.0 jit_solution(15424344154694265073)
XLA Ops:
  0.6 26.5 %shard_map.140 = (bf16[512,256]{1,0:T(8,128)(2,1)}, f32[16,2,128,128]{3,2,1,0:T(8,128)}) custom-call(s32[16]{0:T(128)} %accepted.1, bf16[128,4,256]{2,1,0:T(4,128)(2,1)} %hidden.1, f32[1,2048]{1,0:T(1,128)} %bitcast.3, bf16[2048,256]{1,0:T(8,128)(2,1)} %w_query.1, bf16[2048,256]{1,0:T(8,128)(2,1)} %w_forget.1, bf16[2048,256]{1,0:T(8,128)(2,1)} %w_input.1, ...), custom_call_target="tpu_custom_call" | custom-call | tf_op jit(solution)/shard_map/pallas_call | solution.py:430
  27.1 1.7 %reshape.19 = bf16[128,4,256]{2,1,0:T(4,128)(2,1)} reshape(bf16[512,256]{1,0:T(8,128)(2,1)} %get-tuple-element.4) | data formatting | bytes 524288 | tf_op jit(solution)/shard_map/reshape | solution.py:486
  28.8 3.1 %copy.16 = f32[16,2,128,128]{3,2,1,0:T(8,128)} copy(f32[16,2,128,128]{3,2,1,0:T(8,128)} %get-tuple-element.9) | data formatting | bytes 4194304

commit v2 on v1

--- a/solution.py
+++ b/solution.py
@@ -82,7 +82,7 @@
 def fused_kernel(
     n_kv,
     n_tp,
-    accepted,
+    accepted_hbm,
     hidden,
     gain,
     w_query,
@@ -108,13 +108,13 @@
     state16,
     prev_f_v,
     prev_i_v,
+    counts,
     acc,
     heads_all,
     blocks,
     landed,
     local_sem,
     wo_sem,
-    taken_sem,
     in_send,
     in_recv,
     fwd_send,
@@ -145,6 +145,7 @@
         pltpu.make_async_copy(prev_input, prev_i_v, local_sem.at[2]),
         pltpu.make_async_copy(floor, floor_v, local_sem.at[3]),
         pltpu.make_async_copy(base_state, state, local_sem.at[4]),
+        pltpu.make_async_copy(accepted_hbm, counts, local_sem.at[11]),
         pltpu.make_async_copy(gain, gain_v, local_sem.at[5]),
         pltpu.make_async_copy(head_gain, head_gain_v, local_sem.at[6]),
     ]
@@ -208,7 +209,7 @@
         )
         in_copies[step].start()
 
-    for copy in locals_[1:5]:
+    for copy in locals_[1:6]:
         copy.wait()
     low = floor_v[...]
     row = lax.broadcasted_iota(jnp.int32, (rows, width), 0)
@@ -216,7 +217,7 @@
     seq_of = lax.div(row, props)
     taken_count = jnp.zeros((rows, width), jnp.int32)
     for s in range(seqs):
-        taken_count = jnp.where(seq_of == s, accepted[s], taken_count)
+        taken_count = jnp.where(seq_of == s, counts[s], taken_count)
     live = at < taken_count
     prev_f = low + (1.0 - low) * jax.nn.sigmoid(
         prev_f_v[...].astype(f32).reshape(rows, width)
@@ -259,16 +260,14 @@
             ).astype(bf16)
             both = jnp.dot(left[h], right, preferred_element_type=f32)
             fresh = both[:, HEAD_DIM:] * state[s, h] + both[:, :HEAD_DIM]
-            state[s, h] = fresh
+            taken[s, h] = fresh
             state16[h, :, pl.ds(pl.multiple_of(s * HEAD_DIM, HEAD_DIM), HEAD_DIM)] = fresh.astype(
                 bf16
             )
         return carry
 
     lax.fori_loop(0, seqs, take, 0)
-    taken_copy = pltpu.make_async_copy(state, taken, taken_sem)
-    taken_copy.start()
-    for copy in locals_[5:]:
+    for copy in locals_[6:]:
         copy.wait()
 
     def project(source, block, first):
@@ -398,7 +397,13 @@
     for group in (in_copies, fwd_copies, tp_copies, out_copies, ofwd):
         for copy in group.values():
             copy.wait_send()
-    taken_copy.wait()
+
+
+def write_kernel(flat, taken, out, stored, sem):
+    copy = pltpu.make_async_copy(taken, stored, sem)
+    copy.start()
+    out[...] = flat[...].astype(jnp.float32).reshape(out.shape).astype(out.dtype)
+    copy.wait()
 
 
 def fused(
@@ -427,14 +432,15 @@
     head_local = width // HEAD_DIM
     anywhere = pl.BlockSpec(memory_space=pl.ANY)
     dma = pltpu.SemaphoreType.DMA
+    room = 67043328 - base_state.size * 4 - hidden.size * 2 - 64 * 1024
     out, taken = pl.pallas_call(
         functools.partial(fused_kernel, n_kv, n_tp),
         out_shape=(
-            jax.ShapeDtypeStruct((all_seqs * props, cols), bf16),
-            jax.ShapeDtypeStruct(base_state.shape, f32),
+            pltpu.VMEM((all_seqs * props, cols), bf16),
+            pltpu.VMEM(base_state.shape, f32),
         ),
-        in_specs=[pl.BlockSpec(memory_space=pltpu.SMEM)] + [anywhere] * 12,
-        out_specs=(pl.BlockSpec(memory_space=pltpu.VMEM), anywhere),
+        in_specs=[anywhere] * 13,
+        out_specs=(pl.BlockSpec(memory_space=pltpu.VMEM),) * 2,
         scratch_shapes=[
             pltpu.VMEM(hidden.shape, bf16),
             pltpu.VMEM((n_kv, seqs, props, cols), bf16),
@@ -447,13 +453,13 @@
             pltpu.VMEM((head_local, HEAD_DIM, seqs * HEAD_DIM), bf16),
             pltpu.VMEM(prev_forget.shape, bf16),
             pltpu.VMEM(prev_input.shape, bf16),
+            pltpu.SMEM(accepted.shape, jnp.int32),
             pltpu.VMEM((rows, 4 * width), f32),
             pltpu.VMEM((n_tp, rows, width), bf16),
             pltpu.VMEM((n_kv, rows, cols // 2), bf16),
             pltpu.VMEM((n_kv, 2, rows, cols // 2), bf16),
-            dma((11,)),
-            dma((n_kv,)),
-            dma,
+            dma((12,)),
+            dma((n_kv,)),
             dma((n_kv,)),
             dma((n_kv,)),
             dma((n_kv,)),
@@ -466,7 +472,7 @@
             dma((n_kv,)),
         ],
         compiler_params=pltpu.CompilerParams(
-            collective_id=0, has_side_effects=True, vmem_limit_bytes=56 * 1024 * 1024
+            collective_id=0, has_side_effects=True, vmem_limit_bytes=room
         ),
     )(
         accepted,
@@ -483,7 +489,17 @@
         prev_forget,
         prev_input,
     )
-    return out.reshape(hidden.shape), taken
+    return pl.pallas_call(
+        write_kernel,
+        out_shape=(
+            jax.ShapeDtypeStruct(hidden.shape, bf16),
+            jax.ShapeDtypeStruct(base_state.shape, f32),
+        ),
+        in_specs=[pl.BlockSpec(memory_space=pltpu.VMEM)] * 2,
+        out_specs=(pl.BlockSpec(memory_space=pltpu.VMEM), anywhere),
+        scratch_shapes=[dma],
+        compiler_params=pltpu.CompilerParams(vmem_limit_bytes=16 * 1024 * 1024),
+    )(out, taken)
 
 
 def by_shape(n_kv, n_tp, hidden, *rest):

time: 32.1 us -> 27.9 us (0.87)
  local copies, waits for them, and re-layouts: 4.85 us -> 0 us
  Pallas kernels: 26.5 us -> 27.2 us
    unnamed x1 -> x0, local copies, waits for them, and re-layouts: 3.13 us -> none
    reshape x1 -> x0, local copies, waits for them, and re-layouts: 1.72 us -> none  [fused(): return (out.reshape(hidden.shape), taken)]
    pallas_call x1 -> x2, Pallas kernels: 26.5 us -> 27.2 us  [the longest x1 25.1 us: fused(): pl.pallas_call(functools.partial(fused_kernel, n_kv, n_tp), out_shape=(pl...]
where the time goes in v2:
time: 27.9 us; the launch traced here: 27.8 us
  Pallas kernels  27.2 us (97%)
  between operations  0.64 us (2%)
    pallas_call x1, Pallas kernels, fused(): pl.pallas_call(functools.partial(fused_kernel, n_kv, n_tp), out_shape=(pl...  25.1 us
    pallas_call x1, Pallas kernels, fused(): pl.pallas_call(write_kernel, out_shape=(jax.ShapeDtypeStruct(hidden.shape...  2.03 us

profile of v2, /device:TPU:0, one launch (start us, length us, event | category | flops | bytes accessed | tf_op | source)
XLA Modules:
  0.0 27.8 jit_solution(9791026491029030008)
XLA Ops:
  0.6 25.1 %shard_map.140 = (bf16[512,256]{1,0:T(8,128)(2,1)S(1)}, f32[16,2,128,128]{3,2,1,0:T(8,128)S(1)}) custom-call(s32[16]{0:T(128)} %accepted_hbm.1, bf16[128,4,256]{2,1,0:T(4,128)(2,1)} %hidden.1, f32[1,2048]{1,0:T(1,128)} %bitcast.3, bf16[2048,256]{1,0:T(8,128)(2,1)} %w_query.1, bf16[2048,256]{1,0:T(8,128)(2,1)} %w_forget.1, bf16[2048,256]{1,0:T(8,128)(2,1)} %w_input.1, ...), custom_call_target="tpu_custom_call" | custom-call | tf_op jit(solution)/shard_map/pallas_call | solution.py:436
  25.8 2.0 %shard_map.141 = (bf16[128,4,256]{2,1,0:T(4,128)(2,1)}, f32[16,2,128,128]{3,2,1,0:T(8,128)}) custom-call(bf16[512,256]{1,0:T(8,128)(2,1)S(1)} %get-tuple-element.4.flat, f32[16,2,128,128]{3,2,1,0:T(8,128)S(1)} %get-tuple-element.5.taken), custom_call_target="tpu_custom_call" | custom-call | tf_op jit(solution)/shard_map/pallas_call | solution.py:492

commit v3 on v2

--- a/solution.py
+++ b/solution.py
@@ -163,6 +163,7 @@
         )
         for k in range(n_kv)
     ]
+    locals_[0].start()
     barrier = pltpu.get_barrier_semaphore()
     for step in range(1, n_kv):
         pl.semaphore_signal(
@@ -178,7 +179,7 @@
             device_id={"tp": lax.rem(tp + step, n_tp)},
             device_id_type=pl.DeviceIdType.MESH,
         )
-    for copy in locals_:
+    for copy in locals_[1:]:
         copy.start()
     for copy in w_o_copies:
         copy.start()
@@ -400,10 +401,16 @@
 
 
 def write_kernel(flat, taken, out, stored, sem):
-    copy = pltpu.make_async_copy(taken, stored, sem)
-    copy.start()
+    pieces = sem.shape[0]
+    part = taken.shape[0] // pieces
+    copies = []
+    for piece in range(pieces):
+        some = pl.ds(piece * part, part)
+        copies.append(pltpu.make_async_copy(taken.at[some], stored.at[some], sem.at[piece]))
+        copies[-1].start()
     out[...] = flat[...].astype(jnp.float32).reshape(out.shape).astype(out.dtype)
-    copy.wait()
+    for copy in copies:
+        copy.wait()
 
 
 def fused(
@@ -497,7 +504,7 @@
         ),
         in_specs=[pl.BlockSpec(memory_space=pltpu.VMEM)] * 2,
         out_specs=(pl.BlockSpec(memory_space=pltpu.VMEM), anywhere),
-        scratch_shapes=[dma],
+        scratch_shapes=[dma((4 if seqs % 4 == 0 else 1,))],
         compiler_params=pltpu.CompilerParams(vmem_limit_bytes=16 * 1024 * 1024),
     )(out, taken)
 

time: 27.9 us -> 28 us (level)
  no operation moved by 1% of the time
where the time goes in v3:
time: 28 us; the launch traced here: 27.9 us
  Pallas kernels  27.3 us (98%)
  between operations  0.64 us (2%)
    pallas_call x1, Pallas kernels, fused(): pl.pallas_call(functools.partial(fused_kernel, n_kv, n_tp), out_shape=(pl...  25.2 us
    pallas_call x1, Pallas kernels, fused(): pl.pallas_call(write_kernel, out_shape=(jax.ShapeDtypeStruct(hidden.shape...  2.05 us

profile of v3, /device:TPU:0, one launch (start us, length us, event | category | flops | bytes accessed | tf_op | source)
XLA Modules:
  0.0 27.9 jit_solution(17300422783630610387)
XLA Ops:
  0.6 25.2 %shard_map.140 = (bf16[512,256]{1,0:T(8,128)(2,1)S(1)}, f32[16,2,128,128]{3,2,1,0:T(8,128)S(1)}) custom-call(s32[16]{0:T(128)} %accepted_hbm.1, bf16[128,4,256]{2,1,0:T(4,128)(2,1)} %hidden.1, f32[1,2048]{1,0:T(1,128)} %bitcast.3, bf16[2048,256]{1,0:T(8,128)(2,1)} %w_query.1, bf16[2048,256]{1,0:T(8,128)(2,1)} %w_forget.1, bf16[2048,256]{1,0:T(8,128)(2,1)} %w_input.1, ...), custom_call_target="tpu_custom_call" | custom-call | tf_op jit(solution)/shard_map/pallas_call | solution.py:443
  25.9 2.0 %shard_map.141 = (bf16[128,4,256]{2,1,0:T(4,128)(2,1)}, f32[16,2,128,128]{3,2,1,0:T(8,128)}) custom-call(bf16[512,256]{1,0:T(8,128)(2,1)S(1)} %get-tuple-element.4.flat, f32[16,2,128,128]{3,2,1,0:T(8,128)S(1)} %get-tuple-element.5.taken), custom_call_target="tpu_custom_call" | custom-call | tf_op jit(solution)/shard_map/pallas_call | solution.py:499
